TPU v7x, 32 devices: a whole 2x2x4 slice. The times are simulated.
32 devices in a mesh: fs: 4 (over y, x), tp: 8 (over z, core).
Axes of the slice: x: 2, y: 2, z: 4, core: 2. Of those that a mesh axis runs over, the one named last changes fastest.
Arguments:
- tokens: bfloat16 [4096, 2048], P(('fs', 'tp')), may hold values from -6 to 6
- up_gate: bfloat16 [4096, 5632], P('fs', 'tp'), may hold values from -8 to 8
- up_val: bfloat16 [4096, 5632], P('fs', 'tp'), may hold values from -6 to 6
- gate_weight: bfloat16 [2048, 5632], P('fs', 'tp'), may hold values from -0.125 to 0.125
- val_weight: bfloat16 [2048, 5632], P('fs', 'tp'), may hold values from -0.125 to 0.125
- gate_taps: bfloat16 [3, 5632], P(None, 'tp'), may hold values from -3 to 3
- val_taps: bfloat16 [3, 5632], P(None, 'tp'), may hold values from -3 to 3
- hidden_grad: bfloat16 [4096, 5632], P('fs', 'tp'), may hold values from -6 to 6
Outputs:
- input_grad: bfloat16 [4096, 2048], P(('fs', 'tp'))
- gate_weight_grad: float32 [2048, 5632], P('fs', 'tp')
- val_weight_grad: float32 [2048, 5632], P('fs', 'tp')
- gate_taps_grad: float32 [3, 5632], P(None, 'tp')
- val_taps_grad: float32 [3, 5632], P(None, 'tp')
- gate_row_norms: float32 [2048], P('fs')
- val_row_norms: float32 [2048], P('fs')
- tap_row_norms: float32 [2, 3], replicated
All inputs are finite; a program needn't handle non-finite values.
Results may differ from a plain program's by a relative error of at most 0.017.
Values may be sent and summed in bfloat16 or wider, within the bound.
A program may use at most 128 MiB of HBM per device.

v0:
```python
import functools

import jax
import jax.numpy as jnp
from jax import lax
from jax.experimental import pallas as pl
from jax.experimental.pallas import tpu as pltpu
from jax.sharding import PartitionSpec as P

SEQ = 1024
CORES = 2
MESH = pl.DeviceIdType.MESH
ANY = pl.BlockSpec(memory_space=pl.ANY)
VMEM = pl.BlockSpec(memory_space=pltpu.VMEM)


def hidden_chunks(hidden):
    if hidden % 64:
        return [(0, hidden)]
    sizes = [128] * (hidden // 128) + ([64] if hidden % 128 else [])
    chunks, at = [], 0
    for size in sizes:
        chunks.append((at, size))
        at += size
    return chunks


def piece_shifts(chips):
    return sorted(range(1, chips), key=lambda s: (-min(s, chips - s), s)) + [0]


def stream_steps(n, pieces):
    steps, ready = [], []
    lead = max(0, n - pieces)
    for k in range(lead):
        steps.append((k, k + 1, None))
        ready.append(("chunk", k, len(steps)))
    for j in range(pieces):
        steps.append((lead, n, j))
        if j == pieces - 1:
            for k in range(lead, n):
                ready.append(("chunk", k, len(steps)))
        ready.append(("piece", j, len(steps)))
        if j < pieces - 1 and lead < n - 1:
            for rest in range(j + 1, pieces):
                steps.append((lead, lead + 1, rest))
            ready.append(("chunk", lead, len(steps)))
            lead += 1
    return steps, ready


def conv_rows(group, rows, taps, at, base, size, gate_ref, val_ref, grad_ref, kern_ref, back_ref, tap_ref):
    place = lax.broadcasted_iota(jnp.int32, (group, rows), 1) % SEQ
    lane = lax.broadcasted_iota(jnp.int32, (group, 128), 1)

    def one(index, carry):
        here = pl.multiple_of(at + index * group, group)
        src = pl.ds(here, group)
        kernels = kern_ref[src, :]
        gate_kernel = kernels[:, 0:taps]
        val_kernel = kernels[:, taps : 2 * taps]

        def delayed(field, shift):
            if shift == 0:
                return field
            return jnp.where(place >= shift, pltpu.roll(field, shift, 1), 0.0)

        def advanced(field, shift):
            if shift == 0:
                return field
            return jnp.where(place < SEQ - shift, pltpu.roll(field, rows - shift, 1), 0.0)

        def mixed(fields, kernel):
            total = fields[0] * kernel[:, 0:1]
            for i in range(1, taps):
                total = total + fields[i] * kernel[:, i : i + 1]
            return total

        gate = gate_ref[src, :].astype(jnp.float32)
        val = val_ref[src, :].astype(jnp.float32)
        gate_fields = [delayed(gate, taps - 1 - i) for i in range(taps)]
        val_fields = [delayed(val, taps - 1 - i) for i in range(taps)]
        conv_gate = mixed(gate_fields, gate_kernel)
        conv_val = mixed(val_fields, val_kernel)
        sigmoid = jax.nn.sigmoid(conv_gate)
        scaled = grad_ref[src, :].astype(jnp.float32) * sigmoid
        val_back = scaled * conv_gate
        gate_back = scaled * conv_val * (1.0 + conv_gate * (1.0 - sigmoid))
        row = pl.multiple_of(base + index * group, group)
        back_ref[0, pl.ds(row, group), :] = mixed(
            [advanced(gate_back, taps - 1 - i) for i in range(taps)], gate_kernel
        ).astype(jnp.bfloat16)
        row = pl.multiple_of(base + size + index * group, group)
        back_ref[0, pl.ds(row, group), :] = mixed(
            [advanced(val_back, taps - 1 - i) for i in range(taps)], val_kernel
        ).astype(jnp.bfloat16)
        sums = jnp.zeros((group, 128), jnp.float32)
        for i in range(taps):
            sums = jnp.where(lane == i, jnp.sum(gate_fields[i] * gate_back, axis=1, keepdims=True), sums)
            sums = jnp.where(
                lane == taps + i, jnp.sum(val_fields[i] * val_back, axis=1, keepdims=True), sums
            )
        tap_ref[src, :] = sums
        return carry

    lax.fori_loop(0, size // group, one, 0)


def step_kernel(
    fa, fb, chips, taps,
    tok_ref, up_gate_ref, up_val_ref, gw_ref, vw_ref, kern_ref, grad_ref,
    dx_ref, gate_out, val_out, tap_out, norm_out,
    fg, fv, fh, tok, back, wg, wv, wt, pown, psend, precv, ssend, zrecv, xsend, xrecv,
    gsend, grecv, tapbuf, tapx, normx,
    load_sem, tokx_s, tokx_r, tokz_s, tokz_r, relay_s, tokc_s, tokc_r, w_s, w_r,
    back_s, back_r, pc_s, pc_r, pz_s, pz_r, out_s, out_r, g_s, g_r, tap_s, tap_r, norm_s, norm_r,
):
    f32, bf16 = jnp.float32, jnp.bfloat16
    fs_at = lax.axis_index("fs")
    tp_at = lax.axis_index("tp")
    a_at, b_at = fs_at // fb, fs_at % fb
    z_at, c_at = tp_at // CORES, tp_at % CORES
    hidden, rows = up_gate_ref.shape
    shard, width = tok_ref.shape
    block = gw_ref.shape[1]
    wide = fa * block
    piece = CORES * shard
    chunks = hidden_chunks(hidden)
    shifts = piece_shifts(chips)
    steps, ready = stream_steps(len(chunks), chips)
    tp_size = chips * CORES
    fs_size = fa * fb

    def x_peer(d):
        return (a_at * fb + (b_at + d) % fb, tp_at)

    def y_peer(d):
        return (((a_at + d) % fa) * fb + b_at, tp_at)

    def z_peer(z):
        return (fs_at, z * CORES + c_at)

    core_peer = (fs_at, z_at * CORES + (CORES - 1 - c_at))

    def remote(src, dst, send, recv, peer):
        return pltpu.make_async_remote_copy(
            src_ref=src, dst_ref=dst, send_sem=send, recv_sem=recv, device_id=peer, device_id_type=MESH
        )

    loads = []

    def load(src, dst):
        copy = pltpu.make_async_copy(src, dst, load_sem.at[len(loads)])
        copy.start()
        loads.append(copy)
        return copy

    field_loads = []
    for at, size in chunks:
        cut = pl.ds(at, size)
        field_loads.append(
            [load(s.at[cut], d.at[cut]) for s, d in ((up_gate_ref, fg), (up_val_ref, fv), (grad_ref, fh))]
        )

    def token_columns(d, d_a):
        start = (((a_at + d_a) % fa) * fb + (b_at + d) % fb) * block
        return tok_ref.at[:, pl.ds(pl.multiple_of(start, block), block)]

    def token_rows(z, c):
        return pl.ds(pl.multiple_of((z * CORES + c) * shard, shard), shard)

    mine = token_rows(z_at, c_at)
    tok_loads = [
        load(token_columns(0, d_a), tok.at[0, mine, pl.ds(d_a * block, block)]) for d_a in range(fa)
    ]
    w_loads = [load(gw_ref, wg.at[0]), load(vw_ref, wv.at[0])]

    barrier = pltpu.get_barrier_semaphore()
    peers = [((fs_at + d) % fs_size, tp_at) for d in range(1, fs_size)]
    peers += [(fs_at, (tp_at + d) % tp_size) for d in range(1, tp_size)]
    for peer in peers:
        pl.semaphore_signal(barrier, inc=1, device_id=peer, device_id_type=MESH)
    pl.semaphore_wait(barrier, len(peers))

    sends = []

    def send(copy):
        copy.start()
        sends.append(copy)
        return copy

    tokx = {}
    for d in range(1, fb):
        for d_a in range(fa):
            send(remote(
                token_columns(d, d_a), tok.at[fb - d, mine, pl.ds(d_a * block, block)],
                tokx_s.at[d - 1, d_a], tokx_r.at[fb - d - 1, d_a], x_peer(d),
            ))
            tokx[fb - d, d_a] = sends[-1]
    w_waits = {}
    for d in range(1, fa):
        for i, (src, dst) in enumerate(((gw_ref, wg), (vw_ref, wv))):
            send(remote(src, dst.at[fa - d], w_s.at[d - 1, i], w_r.at[fa - d - 1, i], y_peer(d)))
            w_waits[fa - d, i] = remote(
                src, dst.at[fa - d], w_s.at[d - 1, i], w_r.at[fa - d - 1, i], y_peer(d)
            )

    late = []

    def distance(u, v):
        return jnp.abs(u - v)

    def tok_z(s):
        for j in range(1, chips):
            to = (z_at + j) % chips

            copy = remote(
                tok.at[s, mine], tok.at[s, mine], tokz_s.at[s, j - 1], tokz_r.at[s, z_at], z_peer(to)
            )
            direct = distance(to, z_at) != 2

            @pl.when(direct)
            def _(copy=copy):
                copy.start()

            late.append((direct, copy))
        send(remote(tok.at[s, mine], tok.at[s, mine], tokc_s.at[s, z_at], tokc_r.at[s, z_at], core_peer))

    def tok_arrived(s, source):
        at = token_rows(source, c_at)
        remote(tok.at[s, at], tok.at[s, at], tokz_s.at[s, 0], tokz_r.at[s, source], z_peer(z_at)).wait_recv()

    def to_core(s, source):
        at = token_rows(source, c_at)
        send(remote(tok.at[s, at], tok.at[s, at], tokc_s.at[s, source], tokc_r.at[s, source], core_peer))

    def tok_relay(s):
        for side, step in enumerate((1, -1)):
            source, target = z_at - step, z_at + step
            exists = jnp.logical_and(source >= 0, source < chips)
            both = jnp.logical_and(exists, jnp.logical_and(target >= 0, target < chips))
            source = (source + chips) % chips
            target = (target + chips) % chips
            at = token_rows(source, c_at)
            copy = remote(
                tok.at[s, at], tok.at[s, at], relay_s.at[s, side], tokz_r.at[s, source], z_peer(target)
            )

            @pl.when(exists)
            def _(source=source):
                tok_arrived(s, source)

            @pl.when(both)
            def _(copy=copy):
                copy.start()

            late.append((both, copy))

            forward = remote(
                tok.at[s, at], tok.at[s, at], tokc_s.at[s, source], tokc_r.at[s, source], core_peer
            )

            @pl.when(exists)
            def _(forward=forward):
                forward.start()

            late.append((exists, forward))

    def tok_rest(s):
        for j in range(1, chips):
            source = (z_at + j) % chips
            far = distance(source, z_at) > 1
            at = token_rows(source, c_at)
            forward = remote(
                tok.at[s, at], tok.at[s, at], tokc_s.at[s, source], tokc_r.at[s, source], core_peer
            )

            @pl.when(far)
            def _(source=source, forward=forward):
                tok_arrived(s, source)
                forward.start()

            late.append((far, forward))

    def tok_from_core(s):
        for z in range(chips):
            at = token_rows(z, CORES - 1 - c_at)
            remote(tok.at[s, at], tok.at[s, at], tokc_s.at[s, z], tokc_r.at[s, z], core_peer).wait_recv()

    def lanes(j):
        return pl.ds(pl.multiple_of(((z_at + shifts[j]) % chips) * piece, piece), piece)

    def back_slice(slot, step):
        lo, hi, j = steps[step]
        first = 2 * chunks[lo][0]
        last = 2 * (chunks[hi - 1][0] + chunks[hi - 1][1])
        if j is None:
            return back.at[slot, pl.ds(first, last - first)]
        return back.at[slot, pl.ds(first, last - first), lanes(j)]

    back_waits = {}

    def send_back(step):
        for d in range(1, fb):
            send(remote(
                back_slice(0, step), back_slice(fb - d, step),
                back_s.at[d - 1, step], back_r.at[fb - d - 1, step], x_peer(d),
            ))

    got = [0]

    def await_back(until):
        while got[0] < until:
            step = got[0]
            for s in range(1, fb):
                remote(
                    back_slice(0, step), back_slice(s, step),
                    back_s.at[0, step], back_r.at[s - 1, step], x_peer(1 % fb),
                ).wait_recv()
            got[0] += 1

    if tapbuf.shape[0] > hidden:
        tapbuf[hidden:, :] = jnp.zeros((tapbuf.shape[0] - hidden, 128), f32)

    for copy in tok_loads:
        copy.wait()
    tok_z(0)
    next_step = 0
    after_conv = {0: [lambda: [tok_x_done(), [tok_z(s) for s in range(1, fb)]]]}

    def tok_x_done():
        for s in range(1, fb):
            for d_a in range(fa):
                tokx[s, d_a].wait_recv()

    relays = list(range(fb))
    for k, (at, size) in enumerate(chunks):
        for copy in field_loads[k]:
            copy.wait()
        group = 16 if size % 16 == 0 else 8
        conv_rows(group, rows, taps, at, 2 * at, size, fg, fv, fh, kern_ref, back, tapbuf)
        while next_step < len(steps) and steps[next_step][1] <= k + 1:
            send_back(next_step)
            next_step += 1
        for action in after_conv.get(k, []):
            action()
        if k >= 1 and k % 2 == 0 and relays and k < len(chunks) - 1:
            tok_relay(relays.pop(0))

    tap_t = tapbuf[...].T
    tapx[fs_at] = tap_t[0 : tapx.shape[1], :]
    for d in range(1, fs_size):
        to = ((fs_at + d) % fs_size, tp_at)
        send(remote(tapx.at[fs_at], tapx.at[fs_at], tap_s.at[d - 1], tap_r.at[fs_at], to))

    while relays:
        tok_relay(relays.pop(0))

    def transpose_weights(d):
        for at, size in chunks:
            pair = jnp.concatenate((wg[d, pl.ds(at, size), :], wv[d, pl.ds(at, size), :]), axis=0)
            wt[pl.ds(d * block, block), pl.ds(2 * at, 2 * size)] = pair.T

    for copy in w_loads:
        copy.wait()
    transpose_weights(0)
    for d in range(1, fa):
        for i in range(2):
            w_waits[d, i].wait_recv()
        transpose_weights(d)

    inner = (((1,), (0,)), ((), ()))
    mblock = min(256, wide)

    def partial(r, j):
        right = back[r, :, lanes(j)]

        def one(i, carry):
            at = pl.ds(pl.multiple_of(i * mblock, mblock), mblock)
            out = lax.dot_general(wt[at, :], right, inner, preferred_element_type=f32).astype(bf16)
            own = jnp.where(c_at == 0, out[:, 0:shard], out[:, shard:piece])
            other = jnp.where(c_at == 0, out[:, shard:piece], out[:, 0:shard])
            pown[r, j, at, :] = own
            psend[r, j, at, :] = other
            return carry

        lax.fori_loop(0, wide // mblock, one, 0)
        send(remote(psend.at[r, j], precv.at[r, j], pc_s.at[r, j], pc_r.at[r, j], core_peer))

    def reduce_core(r, j):
        remote(psend.at[r, j], precv.at[r, j], pc_s.at[r, j], pc_r.at[r, j], core_peer).wait_recv()
        total = pown[r, j].astype(f32) + precv[r, j].astype(f32)
        ssend[r, j] = total.astype(bf16)
        if shifts[j]:
            to = (z_at + shifts[j]) % chips
            send(remote(ssend.at[r, j], zrecv.at[r, j], pz_s.at[r, j], pz_r.at[r, j], z_peer(to)))

    def reduce_chips(r):
        total = ssend[r, chips - 1].astype(f32)
        for j in range(chips - 1):
            remote(ssend.at[r, j], zrecv.at[r, j], pz_s.at[r, j], pz_r.at[r, j], z_peer(z_at)).wait_recv()
            total = total + zrecv[r, j].astype(f32)
        return total.astype(bf16).T

    def gradient(k):
        at, size = chunks[k]
        cut = pl.ds(2 * at, 2 * size)
        for d_a in list(range(1, fa)) + [0]:
            cols = slice(d_a * block, (d_a + 1) * block)
            total = lax.dot_general(back[0, cut, :], tok[0, :, cols], inner, preferred_element_type=f32)
            for s in range(1, fb):
                total = total + lax.dot_general(
                    back[s, cut, :], tok[s, :, cols], inner, preferred_element_type=f32
                )
            if d_a:
                gsend[d_a - 1, cut, :] = total.astype(bf16)
                send(remote(
                    gsend.at[d_a - 1, cut], grecv.at[fa - d_a - 1, cut],
                    g_s.at[d_a - 1, k], g_r.at[fa - d_a - 1, k], y_peer(d_a),
                ))
            else:
                gate_out[pl.ds(at, size), :] = total[:size]
                val_out[pl.ds(at, size), :] = total[size:]

    def finish_gradient(k, norms):
        at, size = chunks[k]
        cut = pl.ds(2 * at, 2 * size)
        for s in range(1, fa):
            remote(
                gsend.at[s - 1, cut], grecv.at[s - 1, cut], g_s.at[s - 1, k], g_r.at[s - 1, k], y_peer(1 % fa)
            ).wait_recv()
        new = []
        for i, out in enumerate((gate_out, val_out)):
            rows_at = pl.ds(at, size)
            total = out[rows_at, :]
            for s in range(1, fa):
                total = total + grecv[s - 1, pl.ds(2 * at + i * size, size), :].astype(f32)
            out[rows_at, :] = total
            new.append(norms[i] + jnp.sum(total * total, axis=0, keepdims=True))
        return new

    for j in range(chips):
        partial(0, j)
        if j:
            reduce_core(0, j - 1)
    for s in range(fb):
        tok_rest(s)
    reduce_core(0, chips - 1)
    for s in range(fb):
        tok_from_core(s)

    waiting = []
    for kind, index, until in ready:
        await_back(until)
        if kind == "chunk":
            gradient(index)
            for r, j in waiting:
                reduce_core(r, j)
            waiting = []
        else:
            for r, j in waiting:
                reduce_core(r, j)
            waiting = []
            for r in range(1, fb):
                partial(r, index)
                waiting.append((r, index))

    def place(slot, value):
        for d_a in range(fa):
            start = (((a_at + d_a) % fa) * fb + (b_at + slot) % fb) * block
            dx_ref[:, pl.ds(pl.multiple_of(start, block), block)] = value[:, d_a * block : (d_a + 1) * block]

    place(0, reduce_chips(0))
    for r, j in waiting:
        reduce_core(r, j)

    tap_total = None
    for f in range(fs_size):
        @pl.when(fs_at != f)
        def _(f=f):
            remote(tapx.at[f], tapx.at[f], tap_s.at[0], tap_r.at[f], (fs_at, tp_at)).wait_recv()

        tap_total = tapx[f] if f == 0 else tap_total + tapx[f]
    tap_out[...] = tap_total
    tap_norms = jnp.sum(tap_total * tap_total, axis=1, keepdims=True)

    norms = [jnp.zeros((1, block), f32), jnp.zeros((1, block), f32)]
    n = len(chunks)
    for k in range(max(0, n - 2)):
        norms = finish_gradient(k, norms)

    for r in range(1, fb):
        xsend[r - 1] = reduce_chips(r)
        send(remote(xsend.at[r - 1], xrecv.at[fb - r - 1], out_s.at[r - 1], out_r.at[fb - r - 1], x_peer(r)))

    for k in range(max(0, n - 2), n):
        norms = finish_gradient(k, norms)
    normx[tp_at, 0:1, :] = norms[0]
    normx[tp_at, 1:2, :] = norms[1]
    normx[tp_at, 2 : 2 + 2 * taps, :] = jnp.broadcast_to(tap_norms[0 : 2 * taps], (2 * taps, block))
    for d in range(1, tp_size):
        to = (fs_at, (tp_at + d) % tp_size)
        send(remote(normx.at[tp_at], normx.at[tp_at], norm_s.at[d - 1], norm_r.at[tp_at], to))

    for s in range(1, fb):
        remote(xsend.at[s - 1], xrecv.at[s - 1], out_s.at[s - 1], out_r.at[s - 1], x_peer(1 % fb)).wait_recv()
        place(s, xrecv[s - 1])

    norm_total = None
    for t in range(tp_size):
        @pl.when(tp_at != t)
        def _(t=t):
            remote(normx.at[t], normx.at[t], norm_s.at[0], norm_r.at[t], (fs_at, tp_at)).wait_recv()

        norm_total = normx[t] if t == 0 else norm_total + normx[t]
    norm_out[...] = norm_total

    for copy in sends:
        copy.wait_send()
    for held, copy in late:
        @pl.when(held)
        def _(copy=copy):
            copy.wait_send()


def whole_step(fa, fb, chips, taps, tokens, up_gate, up_val, gate_weight, val_weight, kernels, hidden_grad):
    f32, bf16 = jnp.float32, jnp.bfloat16
    hidden, rows = up_gate.shape
    shard, width = tokens.shape
    block = gate_weight.shape[1]
    wide = fa * block
    fs_size, tp_size = fa * fb, chips * CORES
    chunks = hidden_chunks(hidden)
    n = len(chunks)
    steps, _ = stream_steps(n, chips)
    padded = -(-hidden // 128) * 128
    tap_rows = -(-2 * taps // 8) * 8
    norm_rows = -(-(2 + 2 * taps) // 8) * 8
    dma = pltpu.SemaphoreType.DMA
    xs, ys = max(1, fb - 1), max(1, fa - 1)
    scratch = [
        pltpu.VMEM((hidden, rows), bf16),
        pltpu.VMEM((hidden, rows), bf16),
        pltpu.VMEM((hidden, rows), bf16),
        pltpu.VMEM((fb, rows, wide), bf16),
        pltpu.VMEM((fb, 2 * hidden, rows), bf16),
        pltpu.VMEM((fa, hidden, block), bf16),
        pltpu.VMEM((fa, hidden, block), bf16),
        pltpu.VMEM((wide, 2 * hidden), bf16),
        pltpu.VMEM((fb, chips, wide, shard), bf16),
        pltpu.VMEM((fb, chips, wide, shard), bf16),
        pltpu.VMEM((fb, chips, wide, shard), bf16),
        pltpu.VMEM((fb, chips, wide, shard), bf16),
        pltpu.VMEM((fb, chips, wide, shard), bf16),
        pltpu.VMEM((xs, shard, wide), bf16),
        pltpu.VMEM((xs, shard, wide), bf16),
        pltpu.VMEM((ys, 2 * hidden, block), bf16),
        pltpu.VMEM((ys, 2 * hidden, block), bf16),
        pltpu.VMEM((padded, 128), f32),
        pltpu.VMEM((fs_size, tap_rows, padded), f32),
        pltpu.VMEM((tp_size, norm_rows, block), f32),
        dma((3 * n + fa + 2,)),
        dma((xs, fa)),
        dma((xs, fa)),
        dma((fb, max(1, chips - 1))),
        dma((fb, chips)),
        dma((fb, 2)),
        dma((fb, chips)),
        dma((fb, chips)),
        dma((ys, 2)),
        dma((ys, 2)),
        dma((xs, len(steps))),
        dma((xs, len(steps))),
        dma((fb, chips)),
        dma((fb, chips)),
        dma((fb, chips)),
        dma((fb, chips)),
        dma((xs,)),
        dma((xs,)),
        dma((ys, n)),
        dma((ys, n)),
        dma((max(1, fs_size - 1),)),
        dma((fs_size,)),
        dma((max(1, tp_size - 1),)),
        dma((tp_size,)),
    ]
    return pl.pallas_call(
        functools.partial(step_kernel, fa, fb, chips, taps),
        in_specs=[ANY, ANY, ANY, ANY, ANY, VMEM, ANY],
        out_specs=[VMEM] * 5,
        out_shape=[
            jax.ShapeDtypeStruct((shard, width), bf16),
            jax.ShapeDtypeStruct((hidden, block), f32),
            jax.ShapeDtypeStruct((hidden, block), f32),
            jax.ShapeDtypeStruct((tap_rows, padded), f32),
            jax.ShapeDtypeStruct((norm_rows, block), f32),
        ],
        scratch_shapes=scratch,
        compiler_params=pltpu.CompilerParams(
            collective_id=0, has_side_effects=True, vmem_limit_bytes=60 * 1024 * 1024
        ),
    )(tokens, up_gate, up_val, gate_weight, val_weight, kernels, hidden_grad)


def solution(mesh):
    fs_size, tp_size = mesh.shape["fs"], mesh.shape["tp"]
    fb = max(d for d in range(1, fs_size + 1) if fs_size % d == 0 and d * d <= fs_size)
    fa = fs_size // fb
    chips = tp_size // CORES

    def local(tokens, up_gate, up_val, gate_weight, val_weight, gate_taps, val_taps, hidden_grad):
        taps, hidden = gate_taps.shape
        kernels = jnp.concatenate((gate_taps, val_taps), axis=0).astype(jnp.float32).T
        dx, gate_grad, val_grad, tap_grad, norms = whole_step(
            fa, fb, chips, taps, tokens, up_gate.T, up_val.T, gate_weight.T, val_weight.T,
            kernels, hidden_grad.T,
        )
        return (
            dx,
            gate_grad.T,
            val_grad.T,
            tap_grad[:taps, :hidden],
            tap_grad[taps : 2 * taps, :hidden],
            norms[0],
            norms[1],
            norms[2 : 2 + 2 * taps, 0].reshape(2, taps),
        )

    in_specs = (
        P(("fs", "tp"), None),
        P("fs", "tp"),
        P("fs", "tp"),
        P("fs", "tp"),
        P("fs", "tp"),
        P(None, "tp"),
        P(None, "tp"),
        P("fs", "tp"),
    )
    out_specs = (
        P(("fs", "tp"), None),
        P("fs", "tp"),
        P("fs", "tp"),
        P(None, "tp"),
        P(None, "tp"),
        P("fs"),
        P("fs"),
        P(),
    )
    return jax.shard_map(local, mesh=mesh, in_specs=in_specs, out_specs=out_specs, check_vma=False)
```

profile of v0, /device:TPU:8, one launch (start us, length us, event | category | flops | bytes accessed | tf_op | source)
XLA Modules:
  0.0 112.5 jit_solution(39216056575972784)
XLA Ops:
  0.6 0.7 maximum_convert_fusion
  1.4 0.9 copy.20
  2.3 100.3 %shard_map.143 = (bf16[128,2048]{1,0:T(8,128)(2,1)}, f32[704,512]{1,0:T(8,128)}, f32[704,512]{1,0:T(8,128)}, f32[8,768]{1,0:T(8,128)}, f32[8,512]{1,0:T(8,128)}) custom-call(bf16[128,2048]{1,0:T(8,128)(2,1)} %tok_ref.1, bf16[704,1024]{1,0:T(8,128)(2,1)} %bitcast.13, bf16[704,1024]{1,0:T(8,128)(2,1)} %bitcast.14, bf16[704,512]{1,0:T(8,128)(2,1)} %bitcast.16, ...), custom_call_target="tpu_custom_call" | custom-call | tf_op jit(solution)/shard_map/pallas_call | solution.py:587
  102.5 1.4 %fusion.1 = (f32[1,512]{1,0:T(1,128)}, f32[1,512]{1,0:T(1,128)}) fusion(f32[8,512]{1,0:T(8,128)} %get-tuple-element.17), kind=kLoop, calls=%fused_computation.3 | loop fusion | bytes 8192 | tf_op jit(solution)/shard_map/slice | solution.py:625
  103.9 1.4 %fusion = (f32[3,704]{1,0:T(4,128)}, f32[3,704]{1,0:T(4,128)}) fusion(f32[8,768]{1,0:T(8,128)} %get-tuple-element.16), kind=kLoop, calls=%fused_computation.2 | loop fusion | bytes 33792 | tf_op jit(solution)/shard_map/slice | solution.py:623
  105.3 0.8 slice_reduce_fusion
  106.1 0.6 reshape_squeeze.3
  106.8 1.9 %copy.24 = bf16[128,2048]{1,0:T(8,128)(2,1)} copy(bf16[128,2048]{1,0:T(8,128)(2,1)} %get-tuple-element.30) | data formatting | bytes 1048576
  108.7 0.0 copy-start
  108.7 2.7 %copy.25 = f32[512,704]{0,1:T(8,128)} copy(f32[512,704]{0,1:T(8,128)} %bitcast.11) | data formatting | bytes 2883584
  111.3 0.0 copy-done
  111.4 1.1 copy.26
Async XLA Ops:
  108.7 2.7 %copy-start = (f32[704,512]{1,0:T(8,128)S(1)}, f32[704,512]{1,0:T(8,128)}, u32[]{:S(2)}) copy-start(f32[704,512]{1,0:T(8,128)} %get-tuple-element.15) | copy-start | bytes 4325380
where the time goes:
time: 113 us; the launch traced here: 112 us
  Pallas kernels  100 us (88%)
  local copies, waits for them, and re-layouts  10.8 us (10%)
    pallas_call x1, Pallas kernels, whole_step(): pl.pallas_call(functools.partial(step_kernel, fa, fb, chips, taps), in_sp...  100 us
    unnamed x5, local copies, waits for them, and re-layouts  5.66 us

commit v1 on v0

--- a/solution.py
+++ b/solution.py
@@ -9,15 +9,20 @@
 
 SEQ = 1024
 CORES = 2
+VMEM_LIMIT = 60 * 1024 * 1024
 MESH = pl.DeviceIdType.MESH
 ANY = pl.BlockSpec(memory_space=pl.ANY)
+HBM = pl.BlockSpec(memory_space=pltpu.HBM)
 VMEM = pl.BlockSpec(memory_space=pltpu.VMEM)
 
 
 def hidden_chunks(hidden):
     if hidden % 64:
         return [(0, hidden)]
-    sizes = [128] * (hidden // 128) + ([64] if hidden % 128 else [])
+    units = hidden // 64
+    small = min(5, units)
+    small += (units - small) % 2
+    sizes = [128] * ((units - small) // 2) + [64] * small
     chunks, at = [], 0
     for size in sizes:
         chunks.append((at, size))
@@ -31,21 +36,28 @@
 
 def stream_steps(n, pieces):
     steps, ready = [], []
-    lead = max(0, n - pieces)
+    heads = n - min(3, n)
+    lead = max(0, min(2, heads - 1))
+
+    def rest(k, j):
+        for later in range(j + 1, pieces):
+            steps.append((k, k + 1, later))
+        ready.append(("chunk", k, len(steps)))
+
     for k in range(lead):
         steps.append((k, k + 1, None))
         ready.append(("chunk", k, len(steps)))
-    for j in range(pieces):
+    for j in range(pieces - 1):
         steps.append((lead, n, j))
-        if j == pieces - 1:
-            for k in range(lead, n):
-                ready.append(("chunk", k, len(steps)))
         ready.append(("piece", j, len(steps)))
-        if j < pieces - 1 and lead < n - 1:
-            for rest in range(j + 1, pieces):
-                steps.append((lead, lead + 1, rest))
-            ready.append(("chunk", lead, len(steps)))
+        last = lead + 1 if j < pieces - 3 else heads
+        while j < pieces - 2 and lead < min(last, heads):
+            rest(lead, j)
             lead += 1
+    for k in range(lead, n):
+        steps.append((k, k + 1, pieces - 1))
+        ready.append(("chunk", k, len(steps)))
+    ready.append(("piece", pieces - 1, len(steps)))
     return steps, ready
 
 
@@ -108,12 +120,12 @@
 
 def step_kernel(
     fa, fb, chips, taps,
-    tok_ref, up_gate_ref, up_val_ref, gw_ref, vw_ref, kern_ref, grad_ref,
-    dx_ref, gate_out, val_out, tap_out, norm_out,
+    tok_ref, up_gate_ref, up_val_ref, gw_ref, vw_ref, gate_taps_ref, val_taps_ref, grad_ref,
+    dx_out, gate_done, val_done, tap_out, norm_out,
     fg, fv, fh, tok, back, wg, wv, wt, pown, psend, precv, ssend, zrecv, xsend, xrecv,
-    gsend, grecv, tapbuf, tapx, normx,
+    gsend, grecv, tapbuf, tapx, normx, relayed, gtaps, vtaps, kern_in, kern_ref, dx_ref, gate_out, val_out, held, tap_held, norm_held,
     load_sem, tokx_s, tokx_r, tokz_s, tokz_r, relay_s, tokc_s, tokc_r, w_s, w_r,
-    back_s, back_r, pc_s, pc_r, pz_s, pz_r, out_s, out_r, g_s, g_r, tap_s, tap_r, norm_s, norm_r,
+    back_s, back_r, pc_s, pc_r, pz_s, pz_r, mid_r, out_s, out_r, g_s, g_r, tap_s, tap_r, norm_s, norm_r, save_sem,
 ):
     f32, bf16 = jnp.float32, jnp.bfloat16
     fs_at = lax.axis_index("fs")
@@ -147,7 +159,22 @@
             src_ref=src, dst_ref=dst, send_sem=send, recv_sem=recv, device_id=peer, device_id_type=MESH
         )
 
+    barrier = pltpu.get_barrier_semaphore()
+    peers = [((fs_at + d) % fs_size, tp_at) for d in range(1, fs_size)]
+    peers += [(fs_at, (tp_at + d) % tp_size) for d in range(1, tp_size)]
+    for peer in peers:
+        pl.semaphore_signal(barrier, inc=1, device_id=peer, device_id_type=MESH)
+
     loads = []
+
+    def distance(u, v):
+        return jnp.abs(u - v)
+
+    def may_be_two(shift):
+        return shift == 2 or chips - shift == 2
+
+    def must_be_two(shift):
+        return shift == 2 and chips - shift == 2
 
     def load(src, dst):
         copy = pltpu.make_async_copy(src, dst, load_sem.at[len(loads)])
@@ -155,31 +182,48 @@
         loads.append(copy)
         return copy
 
+    tap_loads = [load(gate_taps_ref, gtaps), load(val_taps_ref, vtaps)]
+    first_loads = [load(tok_ref, held), load(gw_ref, wg.at[0]), load(vw_ref, wv.at[0])]
     field_loads = []
-    for at, size in chunks:
-        cut = pl.ds(at, size)
+    first = chunks[0][1]
+    for cut in [pl.ds(0, first)] + ([pl.ds(first, hidden - first)] if hidden > first else []):
         field_loads.append(
             [load(s.at[cut], d.at[cut]) for s, d in ((up_gate_ref, fg), (up_val_ref, fv), (grad_ref, fh))]
         )
 
-    def token_columns(d, d_a):
+    def token_columns(ref, d, d_a):
         start = (((a_at + d_a) % fa) * fb + (b_at + d) % fb) * block
-        return tok_ref.at[:, pl.ds(pl.multiple_of(start, block), block)]
+        return ref.at[:, pl.ds(pl.multiple_of(start, block), block)]
 
     def token_rows(z, c):
         return pl.ds(pl.multiple_of((z * CORES + c) * shard, shard), shard)
 
     mine = token_rows(z_at, c_at)
     tok_loads = [
-        load(token_columns(0, d_a), tok.at[0, mine, pl.ds(d_a * block, block)]) for d_a in range(fa)
+        load(token_columns(tok_ref, 0, d_a), tok.at[0, mine, pl.ds(d_a * block, block)]) for d_a in range(fa)
     ]
-    w_loads = [load(gw_ref, wg.at[0]), load(vw_ref, wv.at[0])]
-
-    barrier = pltpu.get_barrier_semaphore()
-    peers = [((fs_at + d) % fs_size, tp_at) for d in range(1, fs_size)]
-    peers += [(fs_at, (tp_at + d) % tp_size) for d in range(1, tp_size)]
-    for peer in peers:
-        pl.semaphore_signal(barrier, inc=1, device_id=peer, device_id_type=MESH)
+
+    middle = jnp.logical_and(z_at >= 1, z_at <= chips - 2)
+
+    @pl.when(jnp.logical_not(middle))
+    def _():
+        relayed[...] = jnp.zeros_like(relayed)
+
+    for j, shift in enumerate(shifts):
+        if may_be_two(shift) and not must_be_two(shift):
+            @pl.when(distance((z_at + chips - shift) % chips, z_at) == 2)
+            def _(j=j):
+                zrecv[:, j] = jnp.zeros_like(zrecv[:, j])
+
+    for copy in tap_loads:
+        copy.wait()
+    kern_in[...] = jnp.zeros_like(kern_in)
+    kern_in[0:taps, 0:hidden] = gtaps[...].astype(f32)
+    kern_in[taps : 2 * taps, 0:hidden] = vtaps[...].astype(f32)
+    kern_ref[...] = kern_in[...].T
+
+    for copy in first_loads:
+        copy.wait()
     pl.semaphore_wait(barrier, len(peers))
 
     sends = []
@@ -193,22 +237,20 @@
     for d in range(1, fb):
         for d_a in range(fa):
             send(remote(
-                token_columns(d, d_a), tok.at[fb - d, mine, pl.ds(d_a * block, block)],
+                token_columns(held, d, d_a), tok.at[fb - d, mine, pl.ds(d_a * block, block)],
                 tokx_s.at[d - 1, d_a], tokx_r.at[fb - d - 1, d_a], x_peer(d),
             ))
             tokx[fb - d, d_a] = sends[-1]
     w_waits = {}
     for d in range(1, fa):
-        for i, (src, dst) in enumerate(((gw_ref, wg), (vw_ref, wv))):
+        for i, dst in enumerate((wg, wv)):
+            src = dst.at[0]
             send(remote(src, dst.at[fa - d], w_s.at[d - 1, i], w_r.at[fa - d - 1, i], y_peer(d)))
             w_waits[fa - d, i] = remote(
                 src, dst.at[fa - d], w_s.at[d - 1, i], w_r.at[fa - d - 1, i], y_peer(d)
             )
 
     late = []
-
-    def distance(u, v):
-        return jnp.abs(u - v)
 
     def tok_z(s):
         for j in range(1, chips):
@@ -298,14 +340,14 @@
             return back.at[slot, pl.ds(first, last - first)]
         return back.at[slot, pl.ds(first, last - first), lanes(j)]
 
-    back_waits = {}
 
     def send_back(step):
         for d in range(1, fb):
-            send(remote(
+            copy = remote(
                 back_slice(0, step), back_slice(fb - d, step),
-                back_s.at[d - 1, step], back_r.at[fb - d - 1, step], x_peer(d),
-            ))
+                back_s.at[d - 1], back_r.at[fb - d - 1, step], x_peer(d),
+            )
+            copy.start()
 
     got = [0]
 
@@ -315,7 +357,7 @@
             for s in range(1, fb):
                 remote(
                     back_slice(0, step), back_slice(s, step),
-                    back_s.at[0, step], back_r.at[s - 1, step], x_peer(1 % fb),
+                    back_s.at[0], back_r.at[s - 1, step], x_peer(1 % fb),
                 ).wait_recv()
             got[0] += 1
 
@@ -326,7 +368,7 @@
         copy.wait()
     tok_z(0)
     next_step = 0
-    after_conv = {0: [lambda: [tok_x_done(), [tok_z(s) for s in range(1, fb)]]]}
+    after_conv = {min(1, len(chunks) - 1): [lambda: [tok_x_done(), [tok_z(s) for s in range(1, fb)]]]}
 
     def tok_x_done():
         for s in range(1, fb):
@@ -335,8 +377,9 @@
 
     relays = list(range(fb))
     for k, (at, size) in enumerate(chunks):
-        for copy in field_loads[k]:
-            copy.wait()
+        if k < len(field_loads):
+            for copy in field_loads[k]:
+                copy.wait()
         group = 16 if size % 16 == 0 else 8
         conv_rows(group, rows, taps, at, 2 * at, size, fg, fv, fh, kern_ref, back, tapbuf)
         while next_step < len(steps) and steps[next_step][1] <= k + 1:
@@ -344,39 +387,37 @@
             next_step += 1
         for action in after_conv.get(k, []):
             action()
-        if k >= 1 and k % 2 == 0 and relays and k < len(chunks) - 1:
+        if k == 3:
             tok_relay(relays.pop(0))
 
     tap_t = tapbuf[...].T
     tapx[fs_at] = tap_t[0 : tapx.shape[1], :]
     for d in range(1, fs_size):
         to = ((fs_at + d) % fs_size, tp_at)
-        send(remote(tapx.at[fs_at], tapx.at[fs_at], tap_s.at[d - 1], tap_r.at[fs_at], to))
-
-    while relays:
-        tok_relay(relays.pop(0))
+        copy = remote(tapx.at[fs_at], tapx.at[fs_at], tap_s.at[0], tap_r.at[fs_at], to)
+        copy.start()
 
     def transpose_weights(d):
         for at, size in chunks:
             pair = jnp.concatenate((wg[d, pl.ds(at, size), :], wv[d, pl.ds(at, size), :]), axis=0)
             wt[pl.ds(d * block, block), pl.ds(2 * at, 2 * size)] = pair.T
 
-    for copy in w_loads:
-        copy.wait()
-    transpose_weights(0)
-    for d in range(1, fa):
-        for i in range(2):
-            w_waits[d, i].wait_recv()
-        transpose_weights(d)
-
     inner = (((1,), (0,)), ((), ()))
-    mblock = min(256, wide)
-
-    def partial(r, j):
+    mblock = min(256, block)
+
+    def rows_of(ref, r, j, d):
+        return ref.at[r, j, pl.ds(d * block, block)]
+
+    def core_copy(r, j, d):
+        return remote(
+            rows_of(psend, r, j, d), rows_of(precv, r, j, d), pc_s.at[0], pc_r.at[r, j, d], core_peer
+        )
+
+    def partial(r, j, d):
         right = back[r, :, lanes(j)]
 
         def one(i, carry):
-            at = pl.ds(pl.multiple_of(i * mblock, mblock), mblock)
+            at = pl.ds(pl.multiple_of(d * block + i * mblock, mblock), mblock)
             out = lax.dot_general(wt[at, :], right, inner, preferred_element_type=f32).astype(bf16)
             own = jnp.where(c_at == 0, out[:, 0:shard], out[:, shard:piece])
             other = jnp.where(c_at == 0, out[:, shard:piece], out[:, 0:shard])
@@ -384,23 +425,75 @@
             psend[r, j, at, :] = other
             return carry
 
-        lax.fori_loop(0, wide // mblock, one, 0)
-        send(remote(psend.at[r, j], precv.at[r, j], pc_s.at[r, j], pc_r.at[r, j], core_peer))
-
-    def reduce_core(r, j):
-        remote(psend.at[r, j], precv.at[r, j], pc_s.at[r, j], pc_r.at[r, j], core_peer).wait_recv()
-        total = pown[r, j].astype(f32) + precv[r, j].astype(f32)
-        ssend[r, j] = total.astype(bf16)
-        if shifts[j]:
-            to = (z_at + shifts[j]) % chips
-            send(remote(ssend.at[r, j], zrecv.at[r, j], pz_s.at[r, j], pz_r.at[r, j], z_peer(to)))
-
-    def reduce_chips(r):
-        total = ssend[r, chips - 1].astype(f32)
+        lax.fori_loop(0, block // mblock, one, 0)
+        core_copy(r, j, d).start()
+
+    def relay_copy(r, j, d, side, peer):
+        return remote(
+            rows_of(ssend, r, j, d), relayed.at[r, side, pl.ds(d * block, block)],
+            pz_s.at[r, j, d], mid_r.at[r, side, d], peer,
+        )
+
+    def chip_copy(r, j, d, peer):
+        return remote(
+            rows_of(ssend, r, j, d), rows_of(zrecv, r, j, d), pz_s.at[r, j, d], pz_r.at[r, j, d], peer
+        )
+
+    def reduce_core(r, j, d):
+        core_copy(r, j, d).wait_recv()
+        cut = slice(d * block, (d + 1) * block)
+        total = pown[r, j, cut].astype(f32) + precv[r, j, cut].astype(f32)
+        shift = shifts[j]
+        if chips > 2 and shift in (1, chips - 1):
+            side = 0 if shift == 1 else 1
+
+            @pl.when(middle)
+            def _():
+                relay_copy(r, j, d, side, z_peer(z_at)).wait_recv()
+
+            total = total + relayed[r, side, cut].astype(f32)
+        ssend[r, j, cut] = total.astype(bf16)
+        if shift == 0:
+            return
+        to = (z_at + shift) % chips
+        if not must_be_two(shift):
+            direct = distance(to, z_at) != 2
+            copy = chip_copy(r, j, d, z_peer(to))
+            late.append((direct, copy))
+
+            @pl.when(direct)
+            def _():
+                copy.start()
+        if may_be_two(shift):
+            for side, step in enumerate((1, -1)):
+                through = to == z_at + 2 * step
+                relay = relay_copy(r, j, d, side, z_peer((z_at + step + chips) % chips))
+                late.append((through, relay))
+
+                @pl.when(through)
+                def _(relay=relay):
+                    relay.start()
+
+    def reduce_chips(r, d):
+        cut = slice(d * block, (d + 1) * block)
+        total = ssend[r, chips - 1, cut].astype(f32)
         for j in range(chips - 1):
-            remote(ssend.at[r, j], zrecv.at[r, j], pz_s.at[r, j], pz_r.at[r, j], z_peer(z_at)).wait_recv()
-            total = total + zrecv[r, j].astype(f32)
+            if must_be_two(shifts[j]):
+                continue
+
+            @pl.when(distance((z_at + chips - shifts[j]) % chips, z_at) != 2)
+            def _(j=j):
+                chip_copy(r, j, d, z_peer(z_at)).wait_recv()
+
+            total = total + zrecv[r, j, cut].astype(f32)
         return total.astype(bf16).T
+
+    saves = []
+
+    def save(src, dst):
+        copy = pltpu.make_async_copy(src, dst, save_sem.at[len(saves)])
+        copy.start()
+        saves.append(copy)
 
     def gradient(k):
         at, size = chunks[k]
@@ -414,10 +507,10 @@
                 )
             if d_a:
                 gsend[d_a - 1, cut, :] = total.astype(bf16)
-                send(remote(
+                remote(
                     gsend.at[d_a - 1, cut], grecv.at[fa - d_a - 1, cut],
-                    g_s.at[d_a - 1, k], g_r.at[fa - d_a - 1, k], y_peer(d_a),
-                ))
+                    g_s.at[d_a - 1], g_r.at[fa - d_a - 1, k], y_peer(d_a),
+                ).start()
             else:
                 gate_out[pl.ds(at, size), :] = total[:size]
                 val_out[pl.ds(at, size), :] = total[size:]
@@ -427,7 +520,7 @@
         cut = pl.ds(2 * at, 2 * size)
         for s in range(1, fa):
             remote(
-                gsend.at[s - 1, cut], grecv.at[s - 1, cut], g_s.at[s - 1, k], g_r.at[s - 1, k], y_peer(1 % fa)
+                gsend.at[s - 1, cut], grecv.at[s - 1, cut], g_s.at[s - 1], g_r.at[s - 1, k], y_peer(1 % fa)
             ).wait_recv()
         new = []
         for i, out in enumerate((gate_out, val_out)):
@@ -437,42 +530,81 @@
                 total = total + grecv[s - 1, pl.ds(2 * at + i * size, size), :].astype(f32)
             out[rows_at, :] = total
             new.append(norms[i] + jnp.sum(total * total, axis=0, keepdims=True))
+        if k in (len(chunks) - 4, len(chunks) - 1):
+            low = 0 if k == len(chunks) - 4 or len(chunks) < 4 else chunks[len(chunks) - 3][0]
+            whole = pl.ds(low, at + size - low)
+            save(gate_out.at[whole], gate_done.at[whole])
+            save(val_out.at[whole], val_done.at[whole])
         return new
 
+    transpose_weights(0)
     for j in range(chips):
-        partial(0, j)
-        if j:
-            reduce_core(0, j - 1)
+        partial(0, j, 0)
+        if j == min(1, chips - 1):
+            while relays:
+                tok_relay(relays.pop(0))
+    for d in range(1, fa):
+        for i in range(2):
+            w_waits[d, i].wait_recv()
+        transpose_weights(d)
+        for j in range(chips):
+            partial(0, j, d)
+            if d == 1 and j == 0:
+                reduce_core(0, 0, 0)
+            if j == min(1, chips - 1):
+                reduce_core(0, 0, d)
     for s in range(fb):
         tok_rest(s)
-    reduce_core(0, chips - 1)
+    for j in range(1, chips):
+        for d in range(fa):
+            reduce_core(0, j, d)
     for s in range(fb):
         tok_from_core(s)
 
-    waiting = []
+    def place(slot, d_a, value):
+        start = (((a_at + d_a) % fa) * fb + (b_at + slot) % fb) * block
+        cut = pl.ds(pl.multiple_of(start, block), block)
+        dx_ref[slot, :, d_a * block : (d_a + 1) * block] = value
+        save(dx_ref.at[slot, :, pl.ds(d_a * block, block)], dx_out.at[:, cut])
+
+    norms = [jnp.zeros((1, block), f32), jnp.zeros((1, block), f32)]
+    waiting, finished = [], 0
+
     for kind, index, until in ready:
         await_back(until)
         if kind == "chunk":
             gradient(index)
-            for r, j in waiting:
-                reduce_core(r, j)
+            for item in waiting:
+                reduce_core(*item)
             waiting = []
+            if finished <= index - 3 and until < len(steps) - 2:
+                norms = finish_gradient(finished, norms)
+                finished += 1
         else:
-            for r, j in waiting:
-                reduce_core(r, j)
+            for item in waiting:
+                reduce_core(*item)
             waiting = []
             for r in range(1, fb):
-                partial(r, index)
-                waiting.append((r, index))
-
-    def place(slot, value):
-        for d_a in range(fa):
-            start = (((a_at + d_a) % fa) * fb + (b_at + slot) % fb) * block
-            dx_ref[:, pl.ds(pl.multiple_of(start, block), block)] = value[:, d_a * block : (d_a + 1) * block]
-
-    place(0, reduce_chips(0))
-    for r, j in waiting:
-        reduce_core(r, j)
+                for d in range(fa):
+                    partial(r, index, d)
+                    waiting.append((r, index, d))
+            if index == chips - 2:
+                for item in waiting:
+                    reduce_core(*item)
+                waiting = []
+    for d in range(fa):
+        place(0, d, reduce_chips(0, d))
+    for r in range(1, fb):
+        for d in range(fa):
+            for item in waiting:
+                if item[0] == r and item[2] == d:
+                    reduce_core(*item)
+            cut = pl.ds(d * block, block)
+            xsend[r - 1, :, cut] = reduce_chips(r, d)
+            send(remote(
+                xsend.at[r - 1, :, cut], xrecv.at[fb - r - 1, :, cut],
+                out_s.at[r - 1, d], out_r.at[fb - r - 1, d], x_peer(r),
+            ))
 
     tap_total = None
     for f in range(fs_size):
@@ -481,30 +613,28 @@
             remote(tapx.at[f], tapx.at[f], tap_s.at[0], tap_r.at[f], (fs_at, tp_at)).wait_recv()
 
         tap_total = tapx[f] if f == 0 else tap_total + tapx[f]
-    tap_out[...] = tap_total
+    tap_held[...] = tap_total
+    save(tap_held, tap_out)
     tap_norms = jnp.sum(tap_total * tap_total, axis=1, keepdims=True)
-
-    norms = [jnp.zeros((1, block), f32), jnp.zeros((1, block), f32)]
-    n = len(chunks)
-    for k in range(max(0, n - 2)):
-        norms = finish_gradient(k, norms)
-
-    for r in range(1, fb):
-        xsend[r - 1] = reduce_chips(r)
-        send(remote(xsend.at[r - 1], xrecv.at[fb - r - 1], out_s.at[r - 1], out_r.at[fb - r - 1], x_peer(r)))
-
-    for k in range(max(0, n - 2), n):
+    normx[tp_at, 2 : 2 + 2 * taps, :] = jnp.broadcast_to(tap_norms[0 : 2 * taps], (2 * taps, block))
+
+    for k in range(finished, len(chunks)):
         norms = finish_gradient(k, norms)
     normx[tp_at, 0:1, :] = norms[0]
     normx[tp_at, 1:2, :] = norms[1]
-    normx[tp_at, 2 : 2 + 2 * taps, :] = jnp.broadcast_to(tap_norms[0 : 2 * taps], (2 * taps, block))
     for d in range(1, tp_size):
         to = (fs_at, (tp_at + d) % tp_size)
-        send(remote(normx.at[tp_at], normx.at[tp_at], norm_s.at[d - 1], norm_r.at[tp_at], to))
+        remote(normx.at[tp_at], normx.at[tp_at], norm_s.at[0], norm_r.at[tp_at], to).start()
 
     for s in range(1, fb):
-        remote(xsend.at[s - 1], xrecv.at[s - 1], out_s.at[s - 1], out_r.at[s - 1], x_peer(1 % fb)).wait_recv()
-        place(s, xrecv[s - 1])
+        for d in range(fa):
+            cut = pl.ds(d * block, block)
+            remote(
+                xsend.at[s - 1, :, cut], xrecv.at[s - 1, :, cut],
+                out_s.at[s - 1, d], out_r.at[s - 1, d], x_peer(1 % fb),
+            ).wait_recv()
+            start = (((a_at + d) % fa) * fb + (b_at + s) % fb) * block
+            save(xrecv.at[s - 1, :, cut], dx_out.at[:, pl.ds(pl.multiple_of(start, block), block)])
 
     norm_total = None
     for t in range(tp_size):
@@ -513,17 +643,32 @@
             remote(normx.at[t], normx.at[t], norm_s.at[0], norm_r.at[t], (fs_at, tp_at)).wait_recv()
 
         norm_total = normx[t] if t == 0 else norm_total + normx[t]
-    norm_out[...] = norm_total
-
+    norm_held[...] = norm_total
+    save(norm_held, norm_out)
+
+    for copy in saves:
+        copy.wait()
+    for d in range(1, fb):
+        remote(back.at[0], back.at[fb - d], back_s.at[d - 1], back_r.at[fb - d - 1, 0], x_peer(d)).wait_send()
+    for d in range(1, fa):
+        remote(
+            gsend.at[d - 1], grecv.at[fa - d - 1], g_s.at[d - 1], g_r.at[fa - d - 1, 0], y_peer(d)
+        ).wait_send()
+    remote(psend, precv, pc_s.at[0], pc_r.at[0, 0, 0], core_peer).wait_send()
+    if fs_size > 1:
+        others = tapx.at[pl.ds(0, fs_size - 1)]
+        remote(others, others, tap_s.at[0], tap_r.at[0], x_peer(1 % fb)).wait_send()
+    others = normx.at[pl.ds(0, tp_size - 1)]
+    remote(others, others, norm_s.at[0], norm_r.at[0], core_peer).wait_send()
     for copy in sends:
         copy.wait_send()
-    for held, copy in late:
-        @pl.when(held)
+    for started, copy in late:
+        @pl.when(started)
         def _(copy=copy):
             copy.wait_send()
 
 
-def whole_step(fa, fb, chips, taps, tokens, up_gate, up_val, gate_weight, val_weight, kernels, hidden_grad):
+def whole_step(fa, fb, chips, taps, tokens, up_gate, up_val, gate_weight, val_weight, gate_taps, val_taps, hidden_grad):
     f32, bf16 = jnp.float32, jnp.bfloat16
     hidden, rows = up_gate.shape
     shard, width = tokens.shape
@@ -559,7 +704,18 @@
         pltpu.VMEM((padded, 128), f32),
         pltpu.VMEM((fs_size, tap_rows, padded), f32),
         pltpu.VMEM((tp_size, norm_rows, block), f32),
-        dma((3 * n + fa + 2,)),
+        pltpu.VMEM((fb, 2, wide, shard), bf16),
+        pltpu.VMEM((taps, hidden), bf16),
+        pltpu.VMEM((taps, hidden), bf16),
+        pltpu.VMEM((128, padded), f32),
+        pltpu.VMEM((padded, 128), f32),
+        pltpu.VMEM((1, shard, wide), bf16),
+        pltpu.VMEM((hidden, block), f32),
+        pltpu.VMEM((hidden, block), f32),
+        pltpu.VMEM((shard, width), bf16),
+        pltpu.VMEM((tap_rows, padded), f32),
+        pltpu.VMEM((norm_rows, block), f32),
+        dma((fa + 11,)),
         dma((xs, fa)),
         dma((xs, fa)),
         dma((fb, max(1, chips - 1))),
@@ -569,25 +725,27 @@
         dma((fb, chips)),
         dma((ys, 2)),
         dma((ys, 2)),
+        dma((xs,)),
         dma((xs, len(steps))),
-        dma((xs, len(steps))),
-        dma((fb, chips)),
-        dma((fb, chips)),
-        dma((fb, chips)),
-        dma((fb, chips)),
-        dma((xs,)),
-        dma((xs,)),
+        dma((1,)),
+        dma((fb, chips, fa)),
+        dma((fb, max(1, chips - 1), fa)),
+        dma((fb, max(1, chips - 1), fa)),
+        dma((fb, 2, fa)),
+        dma((xs, fa)),
+        dma((xs, fa)),
+        dma((ys,)),
         dma((ys, n)),
-        dma((ys, n)),
-        dma((max(1, fs_size - 1),)),
+        dma((1,)),
         dma((fs_size,)),
-        dma((max(1, tp_size - 1),)),
+        dma((1,)),
         dma((tp_size,)),
+        dma((fs_size + 6,)),
     ]
     return pl.pallas_call(
         functools.partial(step_kernel, fa, fb, chips, taps),
-        in_specs=[ANY, ANY, ANY, ANY, ANY, VMEM, ANY],
-        out_specs=[VMEM] * 5,
+        in_specs=[HBM] * 8,
+        out_specs=[ANY] * 5,
         out_shape=[
             jax.ShapeDtypeStruct((shard, width), bf16),
             jax.ShapeDtypeStruct((hidden, block), f32),
@@ -597,9 +755,70 @@
         ],
         scratch_shapes=scratch,
         compiler_params=pltpu.CompilerParams(
-            collective_id=0, has_side_effects=True, vmem_limit_bytes=60 * 1024 * 1024
+            collective_id=0, has_side_effects=True, vmem_limit_bytes=VMEM_LIMIT
         ),
-    )(tokens, up_gate, up_val, gate_weight, val_weight, kernels, hidden_grad)
+    )(tokens, up_gate, up_val, gate_weight, val_weight, gate_taps, val_taps, hidden_grad)
+
+
+def results_kernel(
+    taps, hidden, dx_in, gate_in, val_in, tap_in, norm_in,
+    dx_out, gate_out, val_out, gate_tap, val_tap, gate_norm, val_norm, tap_norm,
+    dx, gate, val, tap, norm, gate_tap_held, val_tap_held, gate_norm_held, val_norm_held, tap_norm_held,
+    in_sem, out_sem,
+):
+    half = hidden // 16 * 8
+    parts = [(tap_in, tap, None), (norm_in, norm, None)]
+    for cut in (pl.ds(0, half), pl.ds(half, hidden - half)):
+        for src, held, dst in ((gate_in, gate, gate_out), (val_in, val, val_out)):
+            parts.append((src.at[cut], held.at[cut], dst.at[cut]))
+    parts.append((dx_in, dx, dx_out))
+    ins = [pltpu.make_async_copy(src, held, in_sem.at[i]) for i, (src, held, _) in enumerate(parts)]
+    for copy in ins:
+        copy.start()
+    outs = []
+
+    def out(held, dst):
+        outs.append(pltpu.make_async_copy(held, dst, out_sem.at[len(outs)]))
+        outs[-1].start()
+
+    ins[0].wait()
+    gate_tap_held[...] = tap[0:taps, 0:hidden]
+    val_tap_held[...] = tap[taps : 2 * taps, 0:hidden]
+    ins[1].wait()
+    gate_norm_held[...] = norm[0, :]
+    val_norm_held[...] = norm[1, :]
+    for i in range(2):
+        for t in range(taps):
+            tap_norm_held[i : i + 1, t : t + 1] = norm[2 + i * taps + t : 3 + i * taps + t, 0:1]
+    for held, dst in (
+        (gate_tap_held, gate_tap), (val_tap_held, val_tap), (gate_norm_held, gate_norm),
+        (val_norm_held, val_norm), (tap_norm_held, tap_norm),
+    ):
+        out(held, dst)
+    for i, (_, held, dst) in enumerate(parts):
+        if dst is not None:
+            ins[i].wait()
+        if dst is not None:
+            out(held, dst)
+    for copy in outs:
+        copy.wait()
+
+
+def results(taps, hidden, dx, gate, val, tap, norm):
+    f32 = jnp.float32
+    block = norm.shape[1]
+    small = [((taps, hidden), f32)] * 2 + [((block,), f32)] * 2 + [((2, taps), f32)]
+    return pl.pallas_call(
+        functools.partial(results_kernel, taps, hidden),
+        in_specs=[ANY] * 5,
+        out_specs=[ANY] * 8,
+        out_shape=[jax.ShapeDtypeStruct(v.shape, v.dtype) for v in (dx, gate, val)]
+        + [jax.ShapeDtypeStruct(*kind) for kind in small],
+        scratch_shapes=[pltpu.VMEM(v.shape, v.dtype) for v in (dx, gate, val, tap, norm)]
+        + [pltpu.VMEM(*kind) for kind in small]
+        + [pltpu.SemaphoreType.DMA((7,)), pltpu.SemaphoreType.DMA((10,))],
+        compiler_params=pltpu.CompilerParams(vmem_limit_bytes=VMEM_LIMIT),
+    )(dx, gate, val, tap, norm)
 
 
 def solution(mesh):
@@ -610,21 +829,14 @@
 
     def local(tokens, up_gate, up_val, gate_weight, val_weight, gate_taps, val_taps, hidden_grad):
         taps, hidden = gate_taps.shape
-        kernels = jnp.concatenate((gate_taps, val_taps), axis=0).astype(jnp.float32).T
         dx, gate_grad, val_grad, tap_grad, norms = whole_step(
             fa, fb, chips, taps, tokens, up_gate.T, up_val.T, gate_weight.T, val_weight.T,
-            kernels, hidden_grad.T,
+            gate_taps, val_taps, hidden_grad.T,
         )
-        return (
-            dx,
-            gate_grad.T,
-            val_grad.T,
-            tap_grad[:taps, :hidden],
-            tap_grad[taps : 2 * taps, :hidden],
-            norms[0],
-            norms[1],
-            norms[2 : 2 + 2 * taps, 0].reshape(2, taps),
+        dx, gate_grad, val_grad, gate_tap, val_tap, gate_norm, val_norm, tap_norm = results(
+            taps, hidden, dx, gate_grad, val_grad, tap_grad, norms
         )
+        return dx, gate_grad.T, val_grad.T, gate_tap, val_tap, gate_norm, val_norm, tap_norm
 
     in_specs = (
         P(("fs", "tp"), None),

time: 113 us -> 94.7 us (0.84)
  the two profiles are of different devices: /device:TPU:8 before, /device:TPU:0 now
where the time goes in v1:
time: 94.7 us; the launch traced here: 94.5 us
  Pallas kernels  93.7 us (99%)
    pallas_call x1, Pallas kernels, whole_step(): pl.pallas_call(functools.partial(step_kernel, fa, fb, chips, taps), in_sp...  90.7 us
    pallas_call x1, Pallas kernels, results(): pl.pallas_call(functools.partial(results_kernel, taps, hidden), in_specs=...  3.04 us

profile of v1, /device:TPU:0, one launch (start us, length us, event | category | flops | bytes accessed | tf_op | source)
XLA Modules:
  0.0 94.5 jit_solution(7363014614881308840)
XLA Ops:
  0.6 90.7 %shard_map.143 = (bf16[128,2048]{1,0:T(8,128)(2,1)}, f32[704,512]{1,0:T(8,128)}, f32[704,512]{1,0:T(8,128)}, f32[8,768]{1,0:T(8,128)}, f32[8,512]{1,0:T(8,128)}) custom-call(bf16[128,2048]{1,0:T(8,128)(2,1)} %tok_ref.1, bf16[704,1024]{1,0:T(8,128)(2,1)} %bitcast.7, bf16[704,1024]{1,0:T(8,128)(2,1)} %bitcast.8, bf16[704,512]{1,0:T(8,128)(2,1)} %bitcast.10, ...), custom_call_target="tpu_custom_call" | custom-call | tf_op jit(solution)/shard_map/pallas_call | solution.py:745
  91.3 3.0 %shard_map.144 = (bf16[128,2048]{1,0:T(8,128)(2,1)}, f32[704,512]{1,0:T(8,128)}, f32[704,512]{1,0:T(8,128)}, f32[3,704]{1,0:T(4,128)}, f32[3,704]{1,0:T(4,128)},...) custom-call(bf16[128,2048]{1,0:T(8,128)(2,1)} %get-tuple-element.21.dx_in, f32[704,512]{1,0:T(8,128)} %get-tuple-element.22.gate_in, ...), custom_call_target="tpu_custom_call" | custom-call | tf_op jit(solution)/shard_map/pallas_call | solution.py:811

commit v2 on v1

--- a/solution.py
+++ b/solution.py
@@ -36,7 +36,7 @@
 
 def stream_steps(n, pieces):
     steps, ready = [], []
-    heads = n - min(3, n)
+    heads = n - min(2, n)
     lead = max(0, min(2, heads - 1))
 
     def rest(k, j):
@@ -123,7 +123,7 @@
     tok_ref, up_gate_ref, up_val_ref, gw_ref, vw_ref, gate_taps_ref, val_taps_ref, grad_ref,
     dx_out, gate_done, val_done, tap_out, norm_out,
     fg, fv, fh, tok, back, wg, wv, wt, pown, psend, precv, ssend, zrecv, xsend, xrecv,
-    gsend, grecv, tapbuf, tapx, normx, relayed, gtaps, vtaps, kern_in, kern_ref, dx_ref, gate_out, val_out, held, tap_held, norm_held,
+    gsend, grecv, tapbuf, tapx, normx, relayed, gtaps, vtaps, kern_in, kern_ref, dx_ref, gate_out, val_out, held, tap_held, norm_held, acc,
     load_sem, tokx_s, tokx_r, tokz_s, tokz_r, relay_s, tokc_s, tokc_r, w_s, w_r,
     back_s, back_r, pc_s, pc_r, pz_s, pz_r, mid_r, out_s, out_r, g_s, g_r, tap_s, tap_r, norm_s, norm_r, save_sem,
 ):
@@ -413,12 +413,29 @@
             rows_of(psend, r, j, d), rows_of(precv, r, j, d), pc_s.at[0], pc_r.at[r, j, d], core_peer
         )
 
+    started_early = {}
+
+    def partial_early(r, j, depth):
+        right = back[r, 0:depth, lanes(j)]
+
+        def one(i, carry):
+            at = pl.ds(pl.multiple_of(i * mblock, mblock), mblock)
+            acc[r - 1, at, :] = lax.dot_general(wt[at, 0:depth], right, inner, preferred_element_type=f32)
+            return carry
+
+        lax.fori_loop(0, wide // mblock, one, 0)
+        started_early[r, j] = depth
+
     def partial(r, j, d):
-        right = back[r, :, lanes(j)]
+        depth = started_early.get((r, j), 0)
+        right = back[r, depth:, lanes(j)]
 
         def one(i, carry):
             at = pl.ds(pl.multiple_of(d * block + i * mblock, mblock), mblock)
-            out = lax.dot_general(wt[at, :], right, inner, preferred_element_type=f32).astype(bf16)
+            out = lax.dot_general(wt[at, depth:], right, inner, preferred_element_type=f32)
+            if depth:
+                out = out + acc[r - 1, at, :]
+            out = out.astype(bf16)
             own = jnp.where(c_at == 0, out[:, 0:shard], out[:, shard:piece])
             other = jnp.where(c_at == 0, out[:, shard:piece], out[:, 0:shard])
             pown[r, j, at, :] = own
@@ -574,6 +591,9 @@
         await_back(until)
         if kind == "chunk":
             gradient(index)
+            if chips > 1 and index == len(chunks) - 3 and steps[until][2] == chips - 2:
+                for r in range(1, fb):
+                    partial_early(r, chips - 2, 2 * chunks[index + 1][0])
             for item in waiting:
                 reduce_core(*item)
             waiting = []
@@ -715,6 +735,7 @@
         pltpu.VMEM((shard, width), bf16),
         pltpu.VMEM((tap_rows, padded), f32),
         pltpu.VMEM((norm_rows, block), f32),
+        pltpu.VMEM((xs, wide, CORES * shard), f32),
         dma((fa + 11,)),
         dma((xs, fa)),
         dma((xs, fa)),

time: 94.7 us -> 93.2 us (0.984)
  Pallas kernels: 93.7 us -> 92.2 us
    pallas_call x1, Pallas kernels: 90.7 us -> 89.2 us  [whole_step(): pl.pallas_call(functools.partial(step_kernel, fa, fb, chips, taps), in_sp...]
where the time goes in v2:
time: 93.2 us; the launch traced here: 93.1 us
  Pallas kernels  92.2 us (99%)
    pallas_call x1, Pallas kernels, whole_step(): pl.pallas_call(functools.partial(step_kernel, fa, fb, chips, taps), in_sp...  89.2 us
    pallas_call x1, Pallas kernels, results(): pl.pallas_call(functools.partial(results_kernel, taps, hidden), in_specs=...  3.04 us

profile of v2, /device:TPU:0, one launch (start us, length us, event | category | flops | bytes accessed | tf_op | source)
XLA Modules:
  0.0 93.1 jit_solution(14144575487257590368)
XLA Ops:
  0.6 89.2 %shard_map.143 = (bf16[128,2048]{1,0:T(8,128)(2,1)}, f32[704,512]{1,0:T(8,128)}, f32[704,512]{1,0:T(8,128)}, f32[8,768]{1,0:T(8,128)}, f32[8,512]{1,0:T(8,128)}) custom-call(bf16[128,2048]{1,0:T(8,128)(2,1)} %tok_ref.1, bf16[704,1024]{1,0:T(8,128)(2,1)} %bitcast.7, bf16[704,1024]{1,0:T(8,128)(2,1)} %bitcast.8, bf16[704,512]{1,0:T(8,128)(2,1)} %bitcast.10, ...), custom_call_target="tpu_custom_call" | custom-call | tf_op jit(solution)/shard_map/pallas_call | solution.py:766
  89.9 3.0 %shard_map.144 = (bf16[128,2048]{1,0:T(8,128)(2,1)}, f32[704,512]{1,0:T(8,128)}, f32[704,512]{1,0:T(8,128)}, f32[3,704]{1,0:T(4,128)}, f32[3,704]{1,0:T(4,128)},...) custom-call(bf16[128,2048]{1,0:T(8,128)(2,1)} %get-tuple-element.21.dx_in, f32[704,512]{1,0:T(8,128)} %get-tuple-element.22.gate_in, ...), custom_call_target="tpu_custom_call" | custom-call | tf_op jit(solution)/shard_map/pallas_call | solution.py:832
